TPU v7x, 32 devices: a whole 2x2x4 slice. The times are simulated.
32 devices in a mesh: tp: 4 (over z), dp: 8 (over y, x, core).
Axes of the slice: x: 2, y: 2, z: 4, core: 2. Of those that a mesh axis runs over, the one named last changes fastest.
Arguments:
- tokens: bfloat16 [64, 4096], P(None, 'dp'), may hold values from -6 to 6
- norm_gain: float32 [2, 4096], P(None, 'dp'), may hold values from 0.1 to 1.9
- w_gate: bfloat16 [2, 4096, 3072], P(None, 'dp', 'tp'), may hold values from -0.09375 to 0.09375
- w_value: bfloat16 [2, 4096, 3072], P(None, 'dp', 'tp'), may hold values from -0.09375 to 0.09375
- w_inmap: bfloat16 [2, 4096, 3072], P(None, 'dp', 'tp'), may hold values from -0.09375 to 0.09375
- w_readout: bfloat16 [2, 4096, 3072], P(None, 'dp', 'tp'), may hold values from -0.09375 to 0.09375
- w_step: bfloat16 [2, 4096, 48], P(None, 'dp'), may hold values from -0.09375 to 0.09375
- step_bias: float32 [2, 48], P(None, 'tp'), may hold values from -4 to 1
- decay_log: float32 [2, 48], P(None, 'tp'), may hold values from -1 to 2.5
- skip_gain: float32 [2, 48], P(None, 'tp'), may hold values from 0.5 to 2
- conv_taps: bfloat16 [2, 5, 3, 3072], P(None, None, None, 'tp'), may hold values from -2.5 to 2.5
- gate_gain: float32 [2, 3072], P(None, 'tp'), may hold values from 0.1 to 1.9
- w_project: bfloat16 [2, 3072, 4096], P(None, 'tp', 'dp'), may hold values from -0.109375 to 0.109375
- states: float32 [2, 64, 48, 4096], P(None, 'dp', 'tp'), may hold values from -3 to 3
- recent: bfloat16 [2, 64, 4, 3, 3072], P(None, 'dp', None, None, 'tp'), may hold values from -6 to 6
Outputs:
- next_tokens: bfloat16 [64, 4096], P(None, 'dp')
- next_states: float32 [2, 64, 48, 4096], P(None, 'dp', 'tp')
- next_recent: bfloat16 [2, 64, 4, 3, 3072], P(None, 'dp', None, None, 'tp')
All inputs are finite; a program needn't handle non-finite values.
Results may differ from a plain program's by a relative error of at most 0.014.
Values may be sent and summed in bfloat16 or wider, within the bound.
A program may use at most 64 MiB of HBM per device.

v0:
```python
import jax
import jax.numpy as jnp
from jax import lax
from jax.sharding import PartitionSpec as P

D = 4096
HEADS = 48
HEAD_DIM = 64
STATE = 64
LAYERS = 2


EPS = 1e-06


def run_layers(
    rows_in,
    state_part,
    recent_part,
    norm_gain,
    w_gate,
    w_value,
    w_inmap,
    w_readout,
    w_step,
    step_bias,
    decay_log,
    skip_gain,
    conv_taps,
    gate_gain,
    w_project,
):
    current = rows_in
    state_list = []
    recent_list = []
    for level in range(LAYERS):
        tokens_f = current.astype(jnp.float32)
        part_square = jnp.sum(tokens_f * tokens_f, axis=1)
        gained = (tokens_f * norm_gain[level][None, :]).astype(jnp.bfloat16)

        def project(weight):
            return jnp.dot(gained, weight[level], preferred_element_type=jnp.float32)

        gate_part, value_part, inmap_part, readout_part, step_part, square_sum = (
            lax.psum_scatter(project(w_gate), "dp", scatter_dimension=0, tiled=True),
            lax.psum_scatter(project(w_value), "dp", scatter_dimension=0, tiled=True),
            lax.psum_scatter(project(w_inmap), "dp", scatter_dimension=0, tiled=True),
            lax.psum_scatter(project(w_readout), "dp", scatter_dimension=0, tiled=True),
            lax.psum_scatter(project(w_step), "dp", scatter_dimension=0, tiled=True),
            lax.psum_scatter(part_square, "dp", scatter_dimension=0, tiled=True),
        )
        scale_one = lax.rsqrt(square_sum / D + EPS)[:, None]
        own_rows = gate_part.shape[0]
        columns = gate_part.shape[1]
        head_count = columns // HEAD_DIM
        gate_pre = scale_one * gate_part
        stacked = jnp.stack(
            [scale_one * value_part, scale_one * inmap_part, scale_one * readout_part], axis=1
        ).astype(jnp.bfloat16)
        window = jnp.concatenate([recent_part[level], stacked[:, None]], axis=1)
        taps_sum = jnp.sum(
            window.astype(jnp.float32) * conv_taps[level].astype(jnp.float32)[None], axis=1
        )
        active = jax.nn.silu(taps_sum)
        x_value = active[:, 0].reshape(own_rows, head_count, HEAD_DIM)
        in_map = active[:, 1].reshape(own_rows, head_count, STATE)
        out_map = active[:, 2].reshape(own_rows, head_count, STATE)
        first_head = lax.axis_index("tp") * head_count
        step_raw = lax.dynamic_slice_in_dim(scale_one * step_part, first_head, head_count, 1)
        step_size = jax.nn.softplus(step_raw + step_bias[level][None, :])
        decay_rate = jnp.exp(-step_size * jnp.exp(decay_log[level])[None, :])
        old_state = state_part[level].reshape(own_rows, head_count, HEAD_DIM, STATE)
        fresh = (
            decay_rate[:, :, None, None] * old_state
            + (step_size[:, :, None] * x_value)[:, :, :, None] * in_map[:, :, None, :]
        )
        head_out = (
            jnp.einsum("bhpn,bhn->bhp", fresh, out_map) + skip_gain[level][None, :, None] * x_value
        )
        gated = (
            head_out.reshape(own_rows, columns) * jax.nn.silu(gate_pre) * gate_gain[level][None, :]
        ).astype(jnp.bfloat16)
        all_gated = lax.all_gather(gated, "dp", axis=0, tiled=True)
        gated_f = all_gated.astype(jnp.float32)
        part_two = jnp.sum(gated_f * gated_f, axis=1)
        partial_out = jnp.dot(all_gated, w_project[level], preferred_element_type=jnp.float32)
        out_total, square_two = lax.psum((partial_out, part_two), "tp")
        scale_two = lax.rsqrt(square_two / (HEADS * HEAD_DIM) + EPS)[:, None]
        current = (tokens_f + scale_two * out_total).astype(jnp.bfloat16)
        state_list.append(fresh.reshape(own_rows, head_count, HEAD_DIM * STATE))
        recent_list.append(window[:, 1:])
    return (current, jnp.stack(state_list, axis=0), jnp.stack(recent_list, axis=0))


def per_device(
    tokens,
    norm_gain,
    w_gate,
    w_value,
    w_inmap,
    w_readout,
    w_step,
    step_bias,
    decay_log,
    skip_gain,
    conv_taps,
    gate_gain,
    w_project,
    states,
    recent,
):
    own_count = states.shape[1]
    group_size = lax.axis_size("dp")
    feature_cols = tokens.shape[1]
    half_rows = own_count // 2
    spans = ((0, half_rows), (half_rows, own_count - half_rows))
    by_device = tokens.reshape(group_size, own_count, feature_cols)
    token_parts = []
    state_parts = []
    recent_parts = []
    for span_start, span_count in spans:
        rows_in = by_device[:, span_start : span_start + span_count].reshape(
            group_size * span_count, feature_cols
        )
        result, fresh, kept = run_layers(
            rows_in,
            states[:, span_start : span_start + span_count],
            recent[:, span_start : span_start + span_count],
            norm_gain,
            w_gate,
            w_value,
            w_inmap,
            w_readout,
            w_step,
            step_bias,
            decay_log,
            skip_gain,
            conv_taps,
            gate_gain,
            w_project,
        )
        token_parts.append(result.reshape(group_size, span_count, feature_cols))
        state_parts.append(fresh)
        recent_parts.append(kept)
    next_tokens = jnp.concatenate(token_parts, axis=1).reshape(group_size * own_count, feature_cols)
    return (
        next_tokens,
        jnp.concatenate(state_parts, axis=1),
        jnp.concatenate(recent_parts, axis=1),
    )


def solution(mesh):
    in_specs = (
        P(None, "dp"),
        P(None, "dp"),
        P(None, "dp", "tp"),
        P(None, "dp", "tp"),
        P(None, "dp", "tp"),
        P(None, "dp", "tp"),
        P(None, "dp", None),
        P(None, "tp"),
        P(None, "tp"),
        P(None, "tp"),
        P(None, None, None, "tp"),
        P(None, "tp"),
        P(None, "tp", "dp"),
        P(None, "dp", "tp", None),
        P(None, "dp", None, None, "tp"),
    )
    out_specs = (P(None, "dp"), P(None, "dp", "tp", None), P(None, "dp", None, None, "tp"))
    return jax.shard_map(
        per_device, mesh=mesh, in_specs=in_specs, out_specs=out_specs, check_vma=False
    )
```

profile of v0, /device:TPU:0, one launch (start us, length us, event | category | flops | bytes accessed | tf_op | source)
XLA Modules:
  0.0 372.4 jit_solution(11385981580868170481)
XLA Ops:
  8.0 1.1 multiply_reduce_fusion.9
  9.1 2.0 fusion.38
  11.1 2.1 fusion.42
  14.2 2.1 fusion.40
  21.7 26.2 %all-reduce.25 = (f32[32]{0:T(128)S(1)}, f32[32]{0:T(128)S(1)}, f32[32,48]{1,0:T(8,128)S(1)}, f32[32,48]{1,0:T(8,128)S(1)}) all-reduce(f32[32]{0:T(128)S(1)} %reduce_sum.113, f32[32]{0:T(128)S(1)} %reduce_sum.120, f32[32,48]{1,0:T(8,128)S(1)} %fusion.86, f32[32,48]{1,0:T(8,128)S(1)} %fusion.88), channel_id=2, replica_groups=mesh['tp'=4,'dp'=8] {'dp'}, use_global_device_ids=true, to_apply=%region_1.0.clone | all-reduce | flops 3136 | bytes 25088
  48.0 1.0 slice_convert_fusion
  49.0 1.5 fusion.148
  53.7 2.9 reshape_squeeze.36
  56.7 3.0 reshape_squeeze.42
  61.7 1.1 slice_bitcast_fusion
  62.8 17.3 %all-reduce.39.cloned.1.call-done = (f32[32,768]{1,0:T(8,128)}, f32[32,768]{1,0:T(8,128)}, f32[32,768]{1,0:T(8,128)}, f32[32,768]{1,0:T(8,128)}, f32[32,768]{1,0...) async-done(((f32[32,768]{1,0:T(8,128)}, f32[32,768]{1,0:T(8,128)}, f32[32,768]{1,0:T(8,128)}, f32[32,768]{1,0:T(8,128)}, f32[32,768]{1,0:T(8,128)}, ...) | async-done | bytes 786448
  81.8 1.8 multiply_reduce_fusion.3
  88.9 1.4 reshape.453
  90.3 1.4 mul.707
  93.3 2.1 fusion.6
  99.4 9.2 %all-gather.2 = bf16[8,4,768]{2,1,0:T(4,128)(2,1)} all-gather(bf16[1,4,768]{2,1,0:T(4,128)(2,1)S(1)} %get-tuple-element.92), channel_id=1, replica_groups=mesh['tp'=4,'dp'=8] {'dp'}, dimensions={0}, use_global_device_ids=true | all-gather | bytes 55296 | tf_op jit(solution)/shard_map/all_gather | solution.py:83
  109.5 2.0 fusion.28
  111.5 10.0 %all-gather = bf16[8,4,768]{2,1,0:T(4,128)(2,1)} all-gather(bf16[1,4,768]{2,1,0:T(4,128)(2,1)S(1)} %get-tuple-element.91), channel_id=1, replica_groups=mesh['tp'=4,'dp'=8] {'dp'}, dimensions={0}, use_global_device_ids=true | all-gather | bytes 55296 | tf_op jit(solution)/shard_map/all_gather | solution.py:83
  122.3 2.0 fusion.30
  124.5 2.4 broadcast_multiply_fusion.3
  126.8 2.4 broadcast_multiply_fusion.1
  129.2 11.6 %all-reduce.29 = (f32[32]{0:T(128)S(1)}, f32[32]{0:T(128)S(1)}) all-reduce(f32[32]{0:T(128)S(1)} %multiply_reduce_fusion.5, f32[32]{0:T(128)S(1)} %multiply_reduce_fusion.7), channel_id=1, replica_groups=mesh['tp'=4,'dp'=8] {'tp'}, use_global_device_ids=true, to_apply=%region_31.32 | all-reduce | flops 64 | bytes 512 | tf_op jit(solution)/shard_map/psum | solution.py:87
  141.8 2.9 mul.747
  144.7 2.9 mul.753
  148.3 24.6 %all-reduce.43.cloned.1.call-done = (f32[32,512]{1,0:T(8,128)}, f32[32,512]{1,0:T(8,128)}) async-done(((f32[32,512]{1,0:T(8,128)}, f32[32,512]{1,0:T(8,128)}), (f32[32,512]{1,0:T(8,128)}, f32[32,512]{1,0:T(8,128)})) %all-reduce.43.cloned.1.call-update) | async-done | bytes 131088 | tf_op jit(solution)/shard_map/psum | solution.py:87
  172.9 1.8 fusion.76
  174.6 2.0 fusion.18
  176.6 2.1 fusion.22
  178.8 2.1 fusion.26
  184.3 2.0 fusion.12
  186.3 1.6 fusion.14
  188.8 23.2 %all-reduce.24 = (f32[32]{0:T(128)S(1)}, f32[32]{0:T(128)S(1)}, f32[32,48]{1,0:T(8,128)S(1)}, f32[32,48]{1,0:T(8,128)S(1)}) all-reduce(f32[32]{0:T(128)S(1)} %copy-done.54, f32[32]{0:T(128)} %get-tuple-element.59, f32[32,48]{1,0:T(8,128)S(1)} %fusion.82, f32[32,48]{1,0:T(8,128)} %fusion.84), channel_id=8, replica_groups=mesh['tp'=4,'dp'=8] {'dp'}, use_global_device_ids=true, to_apply=%region_12.13.clone | all-reduce | flops 3136 | bytes 25088
  212.4 1.3 multiply_exponential_fusion.2
  215.1 52.8 %all-reduce.37.cloned.1.call-done = (f32[32,768]{1,0:T(8,128)}, f32[32,768]{1,0:T(8,128)}, f32[32,768]{1,0:T(8,128)}, f32[32,768]{1,0:T(8,128)}, f32[32,768]{1,0...) async-done(((f32[32,768]{1,0:T(8,128)}, f32[32,768]{1,0:T(8,128)}, f32[32,768]{1,0:T(8,128)}, f32[32,768]{1,0:T(8,128)}, f32[32,768]{1,0:T(8,128)}, ...) | async-done | bytes 786448
  269.7 1.0 multiply_reduce_fusion.2
  273.1 1.6 broadcast_multiply_fusion.2
  274.7 2.9 mul.750
  279.8 2.4 broadcast_multiply_fusion
  282.1 2.9 mul.756
  285.1 5.3 %multiply_add_fusion.7 = (f32[1,4,12,4096]{3,1,2,0:T(4,128)}, f32[1,4,12,4096]{3,1,2,0:T(4,128)}, f32[1,4,12,4096]{3,1,2,0:T(4,128)}, f32[1,4,12,4096]{3,1,2,0:T...) fusion(f32[1,4,12,4096]{3,1,2,0:T(4,128)} %mul.747, f32[4,12]{0,1:T(8,128)S(1)} %copy-done.34, ...), kind=kLoop, calls=%fused_computation.56 | loop fusion | flops 1572864 | bytes 11010816 | tf_op jit(solution)/shard_map/add | solution.py:74
  290.4 3.0 reshape_squeeze.39
  294.9 2.1 fusion.4
  300.1 8.3 %all-gather.3 = bf16[8,4,768]{2,1,0:T(4,128)(2,1)S(1)} all-gather(bf16[1,4,768]{2,1,0:T(4,128)(2,1)S(1)} %get-tuple-element.88), channel_id=1, replica_groups=mesh['tp'=4,'dp'=8] {'dp'}, dimensions={0}, use_global_device_ids=true | all-gather | bytes 55296 | tf_op jit(solution)/shard_map/all_gather | solution.py:83
  309.4 9.1 %all-gather.1 = bf16[8,4,768]{2,1,0:T(4,128)(2,1)S(1)} all-gather(bf16[1,4,768]{2,1,0:T(4,128)(2,1)S(1)} %get-tuple-element.87), channel_id=1, replica_groups=mesh['tp'=4,'dp'=8] {'dp'}, dimensions={0}, use_global_device_ids=true | all-gather | bytes 55296 | tf_op jit(solution)/shard_map/all_gather | solution.py:83
  319.6 11.6 %all-reduce.28 = (f32[32]{0:T(128)S(1)}, f32[32]{0:T(128)S(1)}) all-reduce(f32[32]{0:T(128)S(1)} %multiply_reduce_fusion.4, f32[32]{0:T(128)S(1)} %multiply_reduce_fusion.6), channel_id=1, replica_groups=mesh['tp'=4,'dp'=8] {'tp'}, use_global_device_ids=true, to_apply=%region_42.43 | all-reduce | flops 64 | bytes 512 | tf_op jit(solution)/shard_map/psum | solution.py:87
  331.3 3.8 %maximum_maximum_fusion = f32[2,8,12,4096]{3,1,2,0:T(8,128)} fusion(f32[1,4,12,4096]{3,1,2,0:T(4,128)} %get-tuple-element.70, f32[1,4,12,4096]{3,1,2,0:T(4,128)} %get-tuple-element.69, f32[1,4,12,4096]{3,1,2,0:T(4,128)S(1)} %copy-done.10, f32[1,4,12,4096]{3,1,2,0:T(4,128)S(1)} %copy-done.9), kind=kLoop, calls=%fused_computation | loop fusion | flops 2359296 | bytes 6291456 | tf_op jit(solution)/shard_map/concatenate | solution.py:148
  335.2 0.9 maximum_maximum_fusion.1
  336.2 27.1 %all-reduce.41.cloned.1.call-done = (f32[32,512]{1,0:T(8,128)}, f32[32,512]{1,0:T(8,128)}) async-done(((f32[32,512]{1,0:T(8,128)}, f32[32,512]{1,0:T(8,128)}), (f32[32,512]{1,0:T(8,128)}, f32[32,512]{1,0:T(8,128)})) %all-reduce.41.cloned.1.call-update) | async-done | bytes 131088 | tf_op jit(solution)/shard_map/psum | solution.py:87
  (243 shorter events, 49.8 us)
Async XLA Ops:
  7.2 6.1 %copy-start.1 = (bf16[2,512,768]{2,1,0:T(8,128)(2,1)S(1)}, bf16[2,512,768]{2,1,0:T(8,128)(2,1)}, u32[]{:S(2)}) copy-start(bf16[2,512,768]{2,1,0:T(8,128)(2,1)} %param.20) | copy-start | bytes 4718596
  7.2 72.9 %all-reduce.39.cloned.1.call-start = ((), (), s32[]{:S(2)}) async-start(), calls=%async_computation.1 | async-start | bytes 1572864
  8.0 175.3 %copy-start.22 = (f32[1,512]{1,0:T(1,128)}, f32[1,512]{1,0:T(1,128)S(1)}, u32[]{:S(2)}) copy-start(f32[1,512]{1,0:T(1,128)S(1)} %get-tuple-element.89) | copy-start | bytes 6148
  11.1 5.2 %copy-start.4 = (bf16[2,512,768]{2,1,0:T(8,128)(2,1)S(1)}, bf16[2,512,768]{2,1,0:T(8,128)(2,1)}, u32[]{:S(2)}) copy-start(bf16[2,512,768]{2,1,0:T(8,128)(2,1)} %param.18) | copy-start | bytes 4718596
  14.2 3.9 %copy-start.6 = (bf16[2,512,768]{2,1,0:T(8,128)(2,1)S(1)}, bf16[2,512,768]{2,1,0:T(8,128)(2,1)}, u32[]{:S(2)}) copy-start(bf16[2,512,768]{2,1,0:T(8,128)(2,1)} %param.17) | copy-start | bytes 4718596
  17.2 3.2 copy-start.60
  18.1 30.8 %copy-start = (f32[2,8,12,4096]{3,1,2,0:T(8,128)S(1)}, f32[2,8,12,4096]{3,1,2,0:T(8,128)}, u32[]{:S(2)}) copy-start(f32[2,8,12,4096]{3,1,2,0:T(8,128)} %param.28) | copy-start | bytes 9437188
  19.9 153.0 %all-reduce.43.cloned.1.call-start = ((), (), s32[]{:S(2)}) async-start(), calls=%async_computation.3 | async-start | bytes 262144 | tf_op jit(solution)/shard_map/psum | solution.py:87
  47.9 32.2 %copy-start.47 = (f32[4]{0:T(128)}, f32[4]{0:T(128)S(1)}, u32[]{:S(2)}) copy-start(f32[4]{0:T(128)S(1)} %fusion.144) | copy-start | bytes 52
  48.0 32.1 %copy-start.49 = (f32[4]{0:T(128)}, f32[4]{0:T(128)S(1)}, u32[]{:S(2)}) copy-start(f32[4]{0:T(128)S(1)} %fusion.146) | copy-start | bytes 52
  49.0 3.5 copy-start.57
  56.6 4.4 %copy-start.46 = (f32[2,768]{1,0:T(2,128)S(1)}, f32[2,768]{1,0:T(2,128)}, u32[]{:S(2)}) copy-start(f32[2,768]{1,0:T(2,128)} %param.26) | copy-start | bytes 18436
  56.7 36.6 %copy-start.33 = (f32[4,12]{0,1:T(8,128)}, f32[4,12]{0,1:T(8,128)S(1)}, u32[]{:S(2)}) copy-start(f32[4,12]{0,1:T(8,128)S(1)} %copy.62) | copy-start | bytes 580
  91.7 3.8 %copy-start.12 = (f32[4,12,64,64]{3,2,0,1:T(8,128)S(1)}, f32[4,12,64,64]{3,2,0,1:T(8,128)}, u32[]{:S(2)}) copy-start(f32[4,12,64,64]{3,2,0,1:T(8,128)} %reshape_squeeze.42) | copy-start | bytes 2359300
  91.7 3.8 %copy-start.35 = (f32[4,12]{0,1:T(8,128)S(1)}, f32[4,12]{0,1:T(8,128)}, u32[]{:S(2)}) copy-start(f32[4,12]{0,1:T(8,128)} %copy.72) | copy-start | bytes 580
  91.7 3.8 %copy-start.40 = (bf16[4,12,64,1]{2,3,1,0:T(2,128)(2,1)S(1)}, bf16[4,12,64,1]{2,3,1,0:T(2,128)(2,1)}, u32[]{:S(2)}) copy-start(bf16[4,12,64,1]{2,3,1,0:T(2,128)(2,1)} %reshape.453) | copy-start | bytes 18436
  92.6 3.5 copy-start.25
  95.4 3.1 copy-start.44
  95.4 3.1 copy-start.48
  124.5 16.6 %copy-start.16 = (bf16[4,1,3,768]{3,1,2,0:T(2,128)(2,1)S(1)}, bf16[4,1,3,768]{3,1,2,0:T(2,128)(2,1)}, u32[]{:S(2)}) copy-start(bf16[4,1,3,768]{3,1,2,0:T(2,128)(2,1)} %copy-done.15) | copy-start | bytes 55300
  140.8 127.0 %all-reduce.37.cloned.1.call-start = ((), (), s32[]{:S(2)}) async-start(), calls=%async_computation | async-start | bytes 1572864
  147.5 33.4 %copy-start.21 = (f32[32,512]{1,0:T(8,128)S(1)}, f32[32,512]{1,0:T(8,128)}, u32[]{:S(2)}) copy-start(f32[32,512]{1,0:T(8,128)} %reshape.431) | copy-start | bytes 196612
  172.9 8.0 %copy-start.32 = (f32[32,512]{1,0:T(8,128)S(1)}, f32[32,512]{1,0:T(8,128)}, u32[]{:S(2)}) copy-start(f32[32,512]{1,0:T(8,128)} %get-tuple-element.53) | copy-start | bytes 196612
  172.9 8.8 %copy-start.2 = (bf16[2,512,768]{2,1,0:T(8,128)(2,1)S(1)}, bf16[2,512,768]{2,1,0:T(8,128)(2,1)}, u32[]{:S(2)}) copy-start(bf16[2,512,768]{2,1,0:T(8,128)(2,1)} %param.20) | copy-start | bytes 4718596
  176.6 5.9 %copy-start.3 = (bf16[2,512,768]{2,1,0:T(8,128)(2,1)S(1)}, bf16[2,512,768]{2,1,0:T(8,128)(2,1)}, u32[]{:S(2)}) copy-start(bf16[2,512,768]{2,1,0:T(8,128)(2,1)} %param.19) | copy-start | bytes 4718596
  178.8 4.6 %copy-start.5 = (bf16[2,512,768]{2,1,0:T(8,128)(2,1)S(1)}, bf16[2,512,768]{2,1,0:T(8,128)(2,1)}, u32[]{:S(2)}) copy-start(bf16[2,512,768]{2,1,0:T(8,128)(2,1)} %param.18) | copy-start | bytes 4718596
  182.5 3.8 %copy-start.7 = (bf16[2,512,768]{2,1,0:T(8,128)(2,1)S(1)}, bf16[2,512,768]{2,1,0:T(8,128)(2,1)}, u32[]{:S(2)}) copy-start(bf16[2,512,768]{2,1,0:T(8,128)(2,1)} %param.17) | copy-start | bytes 4718596
  183.4 4.5 %copy-start.14 = (bf16[2,512,48]{1,2,0:T(8,128)(2,1)S(1)}, bf16[2,512,48]{1,2,0:T(8,128)(2,1)}, u32[]{:S(2)}) copy-start(bf16[2,512,48]{1,2,0:T(8,128)(2,1)} %param.21) | copy-start | bytes 294916
  183.4 5.4 %copy-start.54 = (f32[32]{0:T(128)S(1)}, f32[32]{0:T(128)}, u32[]{:S(2)}) copy-start(f32[32]{0:T(128)} %get-tuple-element.61) | copy-start | bytes 388
  184.3 3.6 copy-start.23
  184.3 85.4 %copy-start.19 = (f32[5,3,768]{2,0,1:T(8,128)S(1)}, f32[5,3,768]{2,0,1:T(8,128)}, u32[]{:S(2)}) copy-start(f32[5,3,768]{2,0,1:T(8,128)} %get-tuple-element.124) | copy-start | bytes 138244
  212.1 57.5 %copy-start.50 = (f32[4]{0:T(128)}, f32[4]{0:T(128)S(1)}, u32[]{:S(2)}) copy-start(f32[4]{0:T(128)S(1)} %fusion.145) | copy-start | bytes 52
  212.1 57.5 %copy-start.52 = (f32[4]{0:T(128)}, f32[4]{0:T(128)S(1)}, u32[]{:S(2)}) copy-start(f32[4]{0:T(128)S(1)} %fusion.147) | copy-start | bytes 52
  212.2 151.1 %all-reduce.41.cloned.1.call-start = ((), (), s32[]{:S(2)}) async-start(), calls=%async_computation.2 | async-start | bytes 262144 | tf_op jit(solution)/shard_map/psum | solution.py:87
  274.7 2.9 copy-start.24
  274.7 4.4 %copy-start.45 = (f32[4,12]{1,0:T(4,128)S(1)}, f32[4,12]{1,0:T(4,128)}, u32[]{:S(2)}) copy-start(f32[4,12]{1,0:T(4,128)} %get-tuple-element.94) | copy-start | bytes 580
  282.1 2.9 copy-start.34
  282.1 2.9 copy-start.36
  282.1 2.9 copy-start.37
  282.1 2.9 copy-start.38
  290.4 3.0 copy-start.42
  290.4 3.7 copy-start.11
  294.9 2.8 copy-start.55
  297.0 11.5 %copy-start.8 = (bf16[2,768,512]{2,1,0:T(8,128)(2,1)S(1)}, bf16[2,768,512]{2,1,0:T(8,128)(2,1)}, u32[]{:S(2)}) copy-start(bf16[2,768,512]{2,1,0:T(8,128)(2,1)} %param.27) | copy-start | bytes 4718596
  297.6 33.6 %copy-start.9 = (f32[1,4,12,4096]{3,1,2,0:T(4,128)S(1)}, f32[1,4,12,4096]{3,1,2,0:T(4,128)}, u32[]{:S(2)}) copy-start(f32[1,4,12,4096]{3,1,2,0:T(4,128)} %get-tuple-element.67) | copy-start | bytes 2359300
  297.6 33.6 %copy-start.10 = (f32[1,4,12,4096]{3,1,2,0:T(4,128)S(1)}, f32[1,4,12,4096]{3,1,2,0:T(4,128)}, u32[]{:S(2)}) copy-start(f32[1,4,12,4096]{3,1,2,0:T(4,128)} %get-tuple-element.68) | copy-start | bytes 2359300
  331.3 3.9 %copy-start.17 = (bf16[1,4,4,3,768]{4,2,3,1,0:T(4,128)(2,1)S(1)}, bf16[1,4,4,3,768]{4,2,3,1,0:T(4,128)(2,1)}, u32[]{:S(2)}) copy-start(bf16[1,4,4,3,768]{4,2,3,1,0:T(4,128)(2,1)} %fusion.71) | copy-start | bytes 221188
  331.3 3.9 %copy-start.18 = (bf16[1,4,4,3,768]{4,2,3,1,0:T(4,128)(2,1)S(1)}, bf16[1,4,4,3,768]{4,2,3,1,0:T(4,128)(2,1)}, u32[]{:S(2)}) copy-start(bf16[1,4,4,3,768]{4,2,3,1,0:T(4,128)(2,1)} %fusion.75) | copy-start | bytes 221188
  (17 other events, 33.3 us)
Sparse Core Ops, SparseCore 0:
  20.0 60.0 all-reduce.38
  141.0 31.8 all-reduce.42
  212.4 55.4 all-reduce.36
  331.4 31.8 all-reduce.40
where the time goes:
time: 375 us; the launch traced here: 372 us
  waiting for transfers between devices  122 us (33%)
  blocking collectives  109 us (29%)
  local copies, waits for them, and re-layouts  48.2 us (13%)
  other arithmetic  42.4 us (11%)
  matrix products  35.4 us (9%)
  between operations  15 us (4%)
    unnamed x6, waiting for transfers between devices  70.2 us
    psum x2, waiting for transfers between devices, run_layers(): out_total, square_two = lax.psum((partial_out, part_two), 'tp')  51.7 us
    unnamed x2, blocking collectives  49.4 us
    all_gather x4, blocking collectives, run_layers(): all_gated = lax.all_gather(gated, 'dp', axis=0, tiled=True)  36.6 us
    dot_general x20, matrix products, project(): return jnp.dot(gained, weight[level], preferred_element_type=jnp.float32)  24.3 us
    psum x2, blocking collectives, run_layers(): out_total, square_two = lax.psum((partial_out, part_two), 'tp')  23.1 us
    mul x12, local copies, waits for them, and re-layouts, run_layers(): (step_size[:, :, None] * x_value)[:, :, :, None] * in_map[:, :, None, :]  15.3 us
    another operation x4, local copies, waits for them, and re-layouts, run_layers(): old_state = state_part[level].reshape(own_rows, head_count, HEAD_DIM, STATE)  9.65 us
  transfers between devices with their start and end apart: 4, of which 4 were waited for; matrix products, arithmetic and copies ran while one was open for 8% of the time, Pallas kernels for 0%

commit v1 on v0

v1 whole, which is shorter than its diff:
```python
import functools

import jax
import jax.numpy as jnp
from jax import lax
from jax.experimental import pallas as pl
from jax.experimental.pallas import tpu as pltpu
from jax.sharding import PartitionSpec as P

EPS = 1e-06
LANES = 128
MESH = pl.DeviceIdType.MESH
F32 = jnp.float32
BF16 = jnp.bfloat16


def each(count, body):
    if count <= 8:
        for index in range(count):
            body(index)
    else:
        lax.fori_loop(0, count, lambda index, carry: (body(index), carry)[1], 0)


def fold(count, body, start):
    if count <= 8:
        for index in range(count):
            start = body(index, start)
        return start
    return lax.fori_loop(0, count, body, start)


def silu(value):
    return value / (1.0 + jnp.exp(-value))


def halves(value):
    high = value.astype(BF16)
    return high, (value - high.astype(F32)).astype(BF16)


def kernel(
    dims,
    tokens_ref,
    norm_ref,
    params_ref,
    conv_ref,
    value_hbm,
    inmap_hbm,
    readout_hbm,
    gate_hbm,
    step_hbm,
    project_hbm,
    states_hbm,
    tokens_out,
    fresh_hbm,
    u_out,
    w_in,
    w_step,
    w_out,
    state,
    spread,
    gather,
    part_send,
    part_recv,
    extra_send,
    extra_recv,
    gated_all,
    mixed_all,
    dec_ref,
    bm_ref,
    cm_ref,
    wide_ref,
    x_ref,
    in_sem,
    step_sem,
    out_sem,
    state_sem,
    fresh_sem,
    part_ssem,
    part_rsem,
    extra_ssem,
    extra_rsem,
    gated_ssem,
    gated_rsem,
    mixed_ssem,
    mixed_rsem,
):
    layers, dp, tp, own, cols, heads, head_dim, span, features, width = dims
    me = lax.axis_index("dp")
    col = lax.axis_index("tp")
    rows = dp * own

    def peer(k):
        return lax.rem(me + k + 1, dp)

    def column(k):
        return lax.rem(col + k + 1, tp)

    barrier = pltpu.get_barrier_semaphore()
    each(dp - 1, lambda k: pl.semaphore_signal(
        barrier, inc=1, device_id={"dp": peer(k)}, device_id_type=MESH))
    each(tp - 1, lambda k: pl.semaphore_signal(
        barrier, inc=1, device_id={"tp": column(k)}, device_id_type=MESH))

    sources = (inmap_hbm, readout_hbm, value_hbm, gate_hbm)

    def load_step(level):
        return pltpu.make_async_copy(step_hbm.at[level], w_step.at[level], step_sem.at[level])

    def load_in(level, w):
        return pltpu.make_async_copy(
            sources[w].at[level], w_in.at[level, w], in_sem.at[level, w])

    def load_out(level):
        return pltpu.make_async_copy(project_hbm.at[level], w_out.at[level], out_sem.at[level])

    def load_state(level):
        return pltpu.make_async_copy(states_hbm.at[level], state.at[level], state_sem.at[level])

    def save_state(level):
        return pltpu.make_async_copy(state.at[level], fresh_hbm.at[level], fresh_sem.at[level])

    for level in range(layers):
        load_step(level).start()
        for w in range(4):
            load_in(level, w).start()
        load_state(level).start()
        load_out(level).start()

    def send_extra(level, k):
        return pltpu.make_async_remote_copy(
            src_ref=extra_send.at[level, peer(k)],
            dst_ref=extra_recv.at[level, k],
            send_sem=extra_ssem.at[level, k],
            recv_sem=extra_rsem.at[level, k],
            device_id={"dp": peer(k)},
            device_id_type=MESH,
        )

    def send_part(level, w, k):
        return pltpu.make_async_remote_copy(
            src_ref=part_send.at[level, w, peer(k)],
            dst_ref=part_recv.at[level, w, k],
            send_sem=part_ssem.at[level, w, k],
            recv_sem=part_rsem.at[level, w, k],
            device_id={"dp": peer(k)},
            device_id_type=MESH,
        )

    def send_gated(level, k):
        return pltpu.make_async_remote_copy(
            src_ref=gated_all.at[level, me],
            dst_ref=gated_all.at[level, me],
            send_sem=gated_ssem.at[level, k],
            recv_sem=gated_rsem.at[level, k],
            device_id={"dp": peer(k)},
            device_id_type=MESH,
        )

    def send_mixed(level, k):
        return pltpu.make_async_remote_copy(
            src_ref=mixed_all.at[level, col],
            dst_ref=mixed_all.at[level, col],
            send_sem=mixed_ssem.at[level, k],
            recv_sem=mixed_rsem.at[level, k],
            device_id={"tp": column(k)},
            device_id_type=MESH,
        )

    x_ref[...] = tokens_ref[...].astype(F32)
    lane_all = lax.broadcasted_iota(jnp.int32, (rows, LANES), 1)
    lane = lax.broadcasted_iota(jnp.int32, (own, LANES), 1)
    low = lane < head_dim

    def twice(pair, odd):
        turned = pltpu.roll(pair, head_dim, 1)
        return jnp.where(low, turned, pair) if odd else jnp.where(low, pair, turned)

    for level in range(layers):
        x = x_ref[...]
        square = jnp.sum(x * x, axis=1, keepdims=True)
        gained = (x * norm_ref[level][None, :]).astype(BF16)
        load_step(level).wait()
        extra = jnp.dot(gained, w_step[level], preferred_element_type=F32)
        extra = jnp.where(lane_all == LANES - 1, square, extra).reshape(dp, own, LANES)
        high, rest = halves(extra)
        extra_send[level, :, :, :LANES] = high
        extra_send[level, :, :, LANES:] = rest
        if level == 0:
            pl.semaphore_wait(barrier, dp - 1 + tp - 1)
        each(dp - 1, lambda k: send_extra(level, k).start())
        for w in range(4):
            load_in(level, w).wait()
            part = jnp.dot(gained, w_in[level, w], preferred_element_type=F32)
            part_send[level, w] = part.reshape(dp, own, cols).astype(BF16)
            each(dp - 1, lambda k: send_part(level, w, k).start())

        if level == 0:
            step = 256

            def build(index, carry):
                start = pl.multiple_of(index * step, step)
                entry = lax.broadcasted_iota(jnp.int32, (LANES, step), 1) + start
                which = lax.broadcasted_iota(jnp.int32, (LANES, step), 0)
                spread[:, pl.ds(start, step)] = jnp.where(
                    lax.rem(which, head_dim) == entry // span, 1.0, 0.0).astype(BF16)
                entry = lax.broadcasted_iota(jnp.int32, (step, LANES), 0) + start
                which = lax.broadcasted_iota(jnp.int32, (step, LANES), 1)
                gather[pl.ds(start, step), :] = jnp.where(
                    lax.rem(which, head_dim) == entry // span, 1.0, 0.0).astype(BF16)
                return carry

            lax.fori_loop(0, head_dim * span // step, build, 0)

        each(dp - 1, lambda k: send_extra(level, k).wait_recv())

        def add_extra(k, total):
            return total + extra_recv[level, k].astype(F32)

        both = fold(dp - 1, add_extra, extra_send[level, me].astype(F32))
        total = both[:, :LANES] + both[:, LANES:]
        scale = lax.rsqrt(total[:, LANES - 1 :] / features + EPS)
        pick = lax.broadcasted_iota(jnp.int32, (LANES, cols), 0)
        slot = lax.broadcasted_iota(jnp.int32, (LANES, cols), 1)
        chosen = jnp.where(pick == col * heads + slot // head_dim, 1.0, 0.0).astype(BF16)
        high, rest = halves(total * scale)
        raw = jnp.dot(high, chosen, preferred_element_type=F32) + jnp.dot(
            rest, chosen, preferred_element_type=F32)
        raw = raw + params_ref[level, 0:1, :]
        size = jnp.maximum(raw, 0.0) + jnp.log1p(jnp.exp(-jnp.abs(raw)))
        decay = jnp.exp(-size * params_ref[level, 1:2, :])

        def total_part(w):
            each(dp - 1, lambda k: send_part(level, w, k).wait_recv())
            return scale * fold(
                dp - 1,
                lambda k, sum_in: sum_in + part_recv[level, w, k].astype(F32),
                part_send[level, w, me].astype(F32),
            )

        def active(w, place):
            u = total_part(w).astype(BF16)
            u_out[level, :, place * cols : (place + 1) * cols] = u
            return silu(
                conv_ref[level, :, place * cols : (place + 1) * cols]
                + u.astype(F32) * params_ref[level, 4 + place : 5 + place, :])

        bm = active(0, 1)
        cm = active(1, 2)
        for h in range(heads):
            window = slice(h // 2 * LANES, h // 2 * LANES + LANES)
            dec_ref[h] = twice(decay[:, window], h % 2)
            bm_ref[h] = twice(bm[:, window], h % 2)
            cm_ref[h] = twice(cm[:, window], h % 2)
        xv = active(2, 0)
        weighted = size * xv
        for h in range(heads):
            window = slice(h // 2 * LANES, h // 2 * LANES + LANES)
            one = twice(weighted[:, window], h % 2)
            high = one.astype(BF16).astype(F32)
            wide_ref[h * own : (h + 1) * own, :] = jnp.where(low, high, one - high)
        wide = wide_ref[...].astype(BF16)
        load_state(level).wait()
        piece = 512

        def advance(index, y):
            start = pl.multiple_of(index * piece, piece)
            window = pl.ds(start, piece)
            grown = jnp.dot(wide, spread[:, window], preferred_element_type=F32)
            read = []
            for h in range(heads):
                def across(ref):
                    return jnp.concatenate([ref[h]] * (piece // LANES), axis=1)

                fresh = across(dec_ref) * state[level, h, :, window] + (
                    grown[h * own : (h + 1) * own] * across(bm_ref))
                state[level, h, :, window] = fresh
                read.append(fresh * across(cm_ref))
            read = jnp.concatenate(read, axis=0).astype(BF16)
            return y + jnp.dot(read, gather[window, :], preferred_element_type=F32)

        y = lax.fori_loop(
            0, head_dim * span // piece, advance, jnp.zeros((heads * own, LANES), F32))
        save_state(level).start()
        y = jnp.concatenate(
            [
                jnp.where(low, y[h * own : (h + 1) * own], y[(h + 1) * own : (h + 2) * own])
                for h in range(0, heads, 2)
            ],
            axis=1,
        )
        y = y + params_ref[level, 2:3, :] * xv
        gate = total_part(3)
        gated_all[level, me] = (y * silu(gate) * params_ref[level, 3:4, :]).astype(BF16)
        each(dp - 1, lambda k: send_gated(level, k).start())
        load_out(level).wait()
        each(dp - 1, lambda k: send_gated(level, k).wait_recv())
        gated = gated_all[level].astype(F32).reshape(rows, cols)
        square = jnp.sum(gated * gated, axis=1, keepdims=True)
        mixed = jnp.dot(gated.astype(BF16), w_out[level], preferred_element_type=F32)
        high = square.astype(BF16).astype(F32)
        mixed_all[level, col, :, :width] = mixed.astype(BF16)
        mixed_all[level, col, :, width:] = jnp.where(
            lane_all < LANES // 2, high, square - high).astype(BF16)
        each(tp - 1, lambda k: send_mixed(level, k).start())
        each(tp - 1, lambda k: send_mixed(level, k).wait_recv())
        mixed = fold(
            tp,
            lambda k, sum_in: sum_in + mixed_all[level, k].astype(F32),
            jnp.zeros((rows, width + LANES), F32),
        )
        square = mixed[:, width : width + 1] + mixed[:, width + LANES - 1 :]
        scale = lax.rsqrt(square / (cols * tp) + EPS)
        fresh_x = (x_ref[...] + scale * mixed[:, :width]).astype(BF16)
        x_ref[...] = fresh_x.astype(F32)
        if level == layers - 1:
            tokens_out[...] = fresh_x

    for level in range(layers):
        save_state(level).wait()
        each(dp - 1, lambda k: send_extra(level, k).wait_send())
        for w in range(4):
            each(dp - 1, lambda k: send_part(level, w, k).wait_send())
        each(dp - 1, lambda k: send_gated(level, k).wait_send())
        each(tp - 1, lambda k: send_mixed(level, k).wait_send())


def per_device(
    dp,
    tp,
    tokens,
    norm_gain,
    w_gate,
    w_value,
    w_inmap,
    w_readout,
    w_step,
    step_bias,
    decay_log,
    skip_gain,
    conv_taps,
    gate_gain,
    w_project,
    states,
    recent,
):
    layers, own, heads, entries = states.shape
    cols = w_gate.shape[2]
    head_dim = cols // heads
    span = entries // head_dim
    width = tokens.shape[1]
    features = width * dp
    dims = (layers, dp, tp, own, cols, heads, head_dim, span, features, width)
    rows = tokens.shape[0]

    def expand(value):
        return jnp.repeat(value, head_dim, axis=1)[:, None]

    taps = conv_taps.astype(F32)
    params = jnp.concatenate(
        [
            expand(step_bias),
            expand(jnp.exp(decay_log)),
            expand(skip_gain),
            gate_gain[:, None],
            taps[:, -1],
        ],
        axis=1,
    )
    kept = jnp.sum(recent.astype(F32) * taps[:, None, :-1], axis=2).reshape(layers, own, 3 * cols)
    step_weight = jnp.pad(w_step, ((0, 0), (0, 0), (0, LANES - w_step.shape[2])))
    turned = states.transpose(0, 2, 1, 3)
    vmem = pl.BlockSpec(memory_space=pltpu.VMEM)
    anywhere = pl.BlockSpec(memory_space=pl.ANY)
    dma = pltpu.SemaphoreType.DMA
    out_tokens, fresh, u = pl.pallas_call(
        functools.partial(kernel, dims),
        out_shape=(
            jax.ShapeDtypeStruct((rows, width), BF16),
            jax.ShapeDtypeStruct((layers, heads, own, entries), F32),
            jax.ShapeDtypeStruct((layers, own, 3 * cols), BF16),
        ),
        in_specs=[vmem] * 4 + [anywhere] * 7,
        out_specs=(vmem, anywhere, vmem),
        scratch_shapes=[
            pltpu.VMEM((layers, 4, width, cols), BF16),
            pltpu.VMEM((layers, width, LANES), BF16),
            pltpu.VMEM((layers, cols, width), BF16),
            pltpu.VMEM((layers, heads, own, entries), F32),
            pltpu.VMEM((LANES, entries), BF16),
            pltpu.VMEM((entries, LANES), BF16),
            pltpu.VMEM((layers, 4, dp, own, cols), BF16),
            pltpu.VMEM((layers, 4, dp - 1, own, cols), BF16),
            pltpu.VMEM((layers, dp, own, 2 * LANES), BF16),
            pltpu.VMEM((layers, dp - 1, own, 2 * LANES), BF16),
            pltpu.VMEM((layers, dp, own, cols), BF16),
            pltpu.VMEM((layers, tp, rows, width + LANES), BF16),
            pltpu.VMEM((heads, own, LANES), F32),
            pltpu.VMEM((heads, own, LANES), F32),
            pltpu.VMEM((heads, own, LANES), F32),
            pltpu.VMEM((heads * own, LANES), F32),
            pltpu.VMEM((rows, width), F32),
            dma((layers, 4)),
            dma((layers,)),
            dma((layers,)),
            dma((layers,)),
            dma((layers,)),
            dma((layers, 4, dp - 1)),
            dma((layers, 4, dp - 1)),
            dma((layers, dp - 1)),
            dma((layers, dp - 1)),
            dma((layers, dp - 1)),
            dma((layers, dp - 1)),
            dma((layers, tp - 1)),
            dma((layers, tp - 1)),
        ],
        compiler_params=pltpu.CompilerParams(
            collective_id=0, has_side_effects=True, vmem_limit_bytes=50 * 1024 * 1024),
    )(
        tokens,
        norm_gain,
        params,
        kept,
        w_value,
        w_inmap,
        w_readout,
        w_gate,
        step_weight,
        w_project,
        turned,
    )
    next_states = fresh.transpose(0, 2, 1, 3)
    next_recent = jnp.concatenate(
        [recent[:, :, 1:], u.reshape(layers, own, 1, 3, cols)], axis=2)
    return out_tokens, next_states, next_recent


def solution(mesh):
    in_specs = (
        P(None, "dp"),
        P(None, "dp"),
        P(None, "dp", "tp"),
        P(None, "dp", "tp"),
        P(None, "dp", "tp"),
        P(None, "dp", "tp"),
        P(None, "dp", None),
        P(None, "tp"),
        P(None, "tp"),
        P(None, "tp"),
        P(None, None, None, "tp"),
        P(None, "tp"),
        P(None, "tp", "dp"),
        P(None, "dp", "tp", None),
        P(None, "dp", None, None, "tp"),
    )
    out_specs = (P(None, "dp"), P(None, "dp", "tp", None), P(None, "dp", None, None, "tp"))
    body = functools.partial(per_device, mesh.shape["dp"], mesh.shape["tp"])
    return jax.shard_map(
        body, mesh=mesh, in_specs=in_specs, out_specs=out_specs, check_vma=False
    )
```

time: 375 us -> 60.7 us (0.16)
  waiting for transfers between devices: 122 us -> 0 us
  blocking collectives: 109 us -> 0 us
  Pallas kernels: 0 us -> 47.8 us
  local copies, waits for them, and re-layouts: 48.2 us -> 8.48 us
  other arithmetic: 42.4 us -> 3.37 us
  matrix products: 35.4 us -> 0 us
  between operations: 15 us -> 0.82 us
    unnamed x6 -> x0, waiting for transfers between devices: 70.2 us -> none
    psum x2 -> x0, waiting for transfers between devices: 51.7 us -> none  [run_layers(): out_total, square_two = lax.psum((partial_out, part_two), 'tp')]
    unnamed x2 -> x0, blocking collectives: 49.4 us -> none
    pallas_call x0 -> x1, Pallas kernels: none -> 47.8 us  [per_device(): pl.pallas_call(functools.partial(kernel, dims), out_shape=(jax.ShapeDtype...]
    all_gather x4 -> x0, blocking collectives: 36.6 us -> none  [run_layers(): all_gated = lax.all_gather(gated, 'dp', axis=0, tiled=True)]
    dot_general x28 -> x0, matrix products: 35.4 us -> none  [the longest x20 24.3 us: project(): return jnp.dot(gained, weight[level], preferred_element_type=jnp.float32)]
    psum x2 -> x0, blocking collectives: 23.1 us -> none  [run_layers(): out_total, square_two = lax.psum((partial_out, part_two), 'tp')]
    mul x19 -> x0, local copies, waits for them, and re-layouts: 17.8 us -> none  [the longest x12 15.3 us: run_layers(): (step_size[:, :, None] * x_value)[:, :, :, None] * in_map[:, :, None, :]]
  transfers between devices with their start and end apart: 4 -> 0, of which waited for: 4 -> 0; matrix products, arithmetic and copies ran while one was open for 8% -> 0% of each run, Pallas kernels for 0% -> 0%
where the time goes in v1:
time: 60.7 us; the launch traced here: 60.5 us
  Pallas kernels  47.8 us (79%)
  local copies, waits for them, and re-layouts  8.48 us (14%)
  other arithmetic  3.37 us (6%)
  between operations  0.82 us (1%)
    pallas_call x1, Pallas kernels, per_device(): pl.pallas_call(functools.partial(kernel, dims), out_shape=(jax.ShapeDtype...  47.8 us
    unnamed x19, local copies, waits for them, and re-layouts  6.09 us
    reduce_sum x1, other arithmetic, per_device(): jnp.sum(recent.astype(F32) * taps[:, None, :-1], axis=2)  1.41 us

profile of v1, /device:TPU:0, one launch (start us, length us, event | category | flops | bytes accessed | tf_op | source)
XLA Modules:
  0.0 60.5 jit_solution(5216127586641006205)
XLA Ops:
  0.6 0.0 copy-start.7
  0.6 0.0 copy-start.6
  0.7 0.0 copy-start.5
  0.7 0.0 copy-start.2
  0.7 0.0 copy-start.3
  0.7 0.0 copy-start
  0.7 0.9 %copy_convert_fusion = f32[2,5,3,768]{3,2,0,1:T(4,128)S(1)} fusion(bf16[2,5,3,768]{3,0,2,1:T(2,128)(2,1)} %param.25), kind=kLoop, calls=%fused_computation.2 | loop fusion | flops 23040 | bytes 138240 | tf_op jit(solution)/shard_map/convert_element_type | solution.py:360
  1.7 1.4 %multiply_reduce_fusion = f32[2,8,3,768]{3,2,1,0:T(4,128)S(1)} fusion(bf16[2,8,4,3,768]{4,2,3,1,0:T(4,128)(2,1)} %param.29, f32[2,4,3,768]{3,1,2,0:T(4,128)S(1)} %copy.40), kind=kLoop, calls=%fused_computation | loop fusion | flops 405504 | bytes 516096 | tf_op jit(solution)/shard_map/reduce_sum | solution.py:371
  3.1 0.1 reshape.13.conv_ref
  3.2 0.7 %exp.3 = f32[2,12]{1,0:T(2,128)S(1)} exponential(f32[2,12]{1,0:T(2,128)} %param.23) | non-fusion elementwise | bytes 192 | tf_op jit(solution)/shard_map/exp | solution.py:364
  3.9 0.1 broadcast_in_dim.14
  4.0 0.1 broadcast_in_dim_reshape.13
  4.1 0.8 %broadcast_in_dim.13 = f32[2,12,64]{2,1,0:T(8,128)S(1)} broadcast(f32[2,12]{1,0:T(2,128)} %param.22), dimensions={0,1} | broadcast | bytes 6240 | tf_op jit(solution)/shard_map/broadcast_in_dim | solution.py:358
  4.8 0.1 broadcast_in_dim_reshape.12
  4.9 0.0 copy-done.7
  4.9 0.1 broadcast_in_dim.15
  5.0 0.1 broadcast_in_dim_reshape.14
  5.1 0.0 copy-done.6
  5.1 0.1 concatenate.6.params_ref
  5.1 0.0 copy-done.5
  5.2 0.2 copy.41
  5.3 0.1 pad.4.step_hbm
  5.4 0.0 copy-done.2
  5.4 0.0 copy-done.3
  5.4 0.0 copy-done
  5.4 0.0 copy-start.1
  5.4 1.4 %copy-done.1 = bf16[2,512,768]{2,1,0:T(8,128)(2,1)S(1)} copy-done((bf16[2,512,768]{2,1,0:T(8,128)(2,1)S(1)}, bf16[2,512,768]{2,1,0:T(8,128)(2,1)}, u32[]{:S(2)}) %copy-start.1) | copy-done | bytes 1572888
  6.8 0.0 copy-start.4
  6.8 47.8 %shard_map.166 = (bf16[64,512]{1,0:T(8,128)(2,1)S(1)}, f32[2,12,8,4096]{3,2,1,0:T(8,128)}, bf16[2,8,2304]{2,1,0:T(8,128)(2,1)S(1)}) custom-call(bf16[64,512]{1,0:T(8,128)(2,1)S(1)} %copy-done.2, f32[2,512]{1,0:T(2,128)S(1)} %copy-done.3, f32[2,7,768]{2,1,0:T(8,128)S(1)} %concatenate.6.params_ref, f32[2,8,2304]{2,1,0:T(8,128)S(1)} %reshape.13.conv_ref, ...), custom_call_target="tpu_custom_call" | custom-call | tf_op jit(solution)/shard_map/pallas_call | solution.py:377
  54.7 0.1 copy.42
  54.8 0.0 copy-done.4
  54.8 0.2 slice.11
  55.0 1.0 %pad_maximum_fusion = bf16[2,8,4,3,768]{4,2,3,1,0:T(4,128)(2,1)} fusion(bf16[2,8,1,3,768]{4,2,3,1,0:T(2,128)(2,1)S(1)} %copy.42, bf16[2,8,3,3,768]{4,2,3,1,0:T(4,128)(2,1)S(1)} %slice.11), kind=kLoop, calls=%fused_computation.1 | loop fusion | flops 589824 | bytes 589824 | tf_op jit(solution)/shard_map/concatenate | solution.py:434
  56.0 0.6 %copy.46 = bf16[64,512]{1,0:T(8,128)(2,1)} copy(bf16[64,512]{1,0:T(8,128)(2,1)S(1)} %get-tuple-element.12) | data formatting | bytes 131072
  56.6 3.9 %copy.47 = f32[2,8,12,4096]{3,1,2,0:T(8,128)} copy(f32[2,8,12,4096]{3,1,2,0:T(8,128)} %bitcast.6) | data formatting | bytes 6291456
  (4 shorter events, 0.1 us)
Async XLA Ops:
  0.6 4.3 %copy-start.7 = (f32[2,12]{1,0:T(2,128)S(1)}, f32[2,12]{1,0:T(2,128)}, u32[]{:S(2)}) copy-start(f32[2,12]{1,0:T(2,128)} %param.24) | copy-start | bytes 292
  0.6 4.4 %copy-start.6 = (f32[2,768]{1,0:T(2,128)S(1)}, f32[2,768]{1,0:T(2,128)}, u32[]{:S(2)}) copy-start(f32[2,768]{1,0:T(2,128)} %param.26) | copy-start | bytes 18436
  0.7 4.5 %copy-start.5 = (bf16[2,512,48]{1,2,0:T(8,128)(2,1)S(1)}, bf16[2,512,48]{1,2,0:T(8,128)(2,1)}, u32[]{:S(2)}) copy-start(bf16[2,512,48]{1,2,0:T(8,128)(2,1)} %param.21) | copy-start | bytes 294916
  0.7 4.7 %copy-start.2 = (bf16[64,512]{1,0:T(8,128)(2,1)S(1)}, bf16[64,512]{1,0:T(8,128)(2,1)}, u32[]{:S(2)}) copy-start(bf16[64,512]{1,0:T(8,128)(2,1)} %tokens_ref.1) | copy-start | bytes 196612
  0.7 4.7 %copy-start.3 = (f32[2,512]{1,0:T(2,128)S(1)}, f32[2,512]{1,0:T(2,128)}, u32[]{:S(2)}) copy-start(f32[2,512]{1,0:T(2,128)} %norm_ref.1) | copy-start | bytes 12292
  0.7 4.7 %copy-start = (bf16[2,512,768]{2,1,0:T(8,128)(2,1)S(1)}, bf16[2,512,768]{2,1,0:T(8,128)(2,1)}, u32[]{:S(2)}) copy-start(bf16[2,512,768]{2,1,0:T(8,128)(2,1)} %value_hbm.1) | copy-start | bytes 4718596
  5.4 1.4 %copy-start.1 = (bf16[2,512,768]{2,1,0:T(8,128)(2,1)S(1)}, bf16[2,512,768]{2,1,0:T(8,128)(2,1)}, u32[]{:S(2)}) copy-start(bf16[2,512,768]{2,1,0:T(8,128)(2,1)} %inmap_hbm.1) | copy-start | bytes 4718596
  6.8 48.0 %copy-start.4 = (bf16[2,8,4,3,768]{4,2,3,1,0:T(4,128)(2,1)S(1)}, bf16[2,8,4,3,768]{4,2,3,1,0:T(4,128)(2,1)}, u32[]{:S(2)}) copy-start(bf16[2,8,4,3,768]{4,2,3,1,0:T(4,128)(2,1)} %param.29) | copy-start | bytes 884740

commit v2 on v1

--- a/solution.py
+++ b/solution.py
@@ -43,8 +43,12 @@
     dims,
     tokens_ref,
     norm_ref,
-    params_ref,
-    conv_ref,
+    bias_ref,
+    rate_ref,
+    skip_ref,
+    gain_ref,
+    taps_ref,
+    recent_ref,
     value_hbm,
     inmap_hbm,
     readout_hbm,
@@ -53,7 +57,7 @@
     project_hbm,
     states_hbm,
     tokens_out,
-    fresh_hbm,
+    fresh_out,
     u_out,
     w_in,
     w_step,
@@ -67,6 +71,10 @@
     extra_recv,
     gated_all,
     mixed_all,
+    square_all,
+    conv_ref,
+    params_ref,
+    chosen_ref,
     dec_ref,
     bm_ref,
     cm_ref,
@@ -76,7 +84,6 @@
     step_sem,
     out_sem,
     state_sem,
-    fresh_sem,
     part_ssem,
     part_rsem,
     extra_ssem,
@@ -85,6 +92,8 @@
     gated_rsem,
     mixed_ssem,
     mixed_rsem,
+    square_ssem,
+    square_rsem,
 ):
     layers, dp, tp, own, cols, heads, head_dim, span, features, width = dims
     me = lax.axis_index("dp")
@@ -106,7 +115,7 @@
     sources = (inmap_hbm, readout_hbm, value_hbm, gate_hbm)
 
     def load_step(level):
-        return pltpu.make_async_copy(step_hbm.at[level], w_step.at[level], step_sem.at[level])
+        return pltpu.make_async_copy(step_hbm.at[level], w_step.at[level, : step_hbm.shape[1]], step_sem.at[level])
 
     def load_in(level, w):
         return pltpu.make_async_copy(
@@ -118,9 +127,8 @@
     def load_state(level):
         return pltpu.make_async_copy(states_hbm.at[level], state.at[level], state_sem.at[level])
 
-    def save_state(level):
-        return pltpu.make_async_copy(state.at[level], fresh_hbm.at[level], fresh_sem.at[level])
-
+    filled = step_hbm.shape[1]
+    w_step[:, filled:] = jnp.zeros((layers, LANES - filled, width), BF16)
     for level in range(layers):
         load_step(level).start()
         for w in range(4):
@@ -168,6 +176,16 @@
             device_id_type=MESH,
         )
 
+    def send_square(level, k):
+        return pltpu.make_async_remote_copy(
+            src_ref=square_all.at[level, col],
+            dst_ref=square_all.at[level, col],
+            send_sem=square_ssem.at[level, k],
+            recv_sem=square_rsem.at[level, k],
+            device_id={"tp": column(k)},
+            device_id_type=MESH,
+        )
+
     x_ref[...] = tokens_ref[...].astype(F32)
     lane_all = lax.broadcasted_iota(jnp.int32, (rows, LANES), 1)
     lane = lax.broadcasted_iota(jnp.int32, (own, LANES), 1)
@@ -182,7 +200,8 @@
         square = jnp.sum(x * x, axis=1, keepdims=True)
         gained = (x * norm_ref[level][None, :]).astype(BF16)
         load_step(level).wait()
-        extra = jnp.dot(gained, w_step[level], preferred_element_type=F32)
+        extra = lax.dot_general(
+            gained, w_step[level], (((1,), (1,)), ((), ())), preferred_element_type=F32)
         extra = jnp.where(lane_all == LANES - 1, square, extra).reshape(dp, own, LANES)
         high, rest = halves(extra)
         extra_send[level, :, :, :LANES] = high
@@ -212,6 +231,26 @@
                 return carry
 
             lax.fori_loop(0, head_dim * span // step, build, 0)
+            pick = lax.broadcasted_iota(jnp.int32, (LANES, cols), 0)
+            slot = lax.broadcasted_iota(jnp.int32, (LANES, cols), 1)
+            chosen_ref[...] = jnp.where(
+                pick == col * heads + slot // head_dim, 1.0, 0.0).astype(BF16)
+            pick = lax.broadcasted_iota(jnp.int32, (heads, cols), 0)
+            slot = lax.broadcasted_iota(jnp.int32, (heads, cols), 1)
+            wider = jnp.where(pick == slot // head_dim, 1.0, 0.0)
+            for place, value in enumerate((bias_ref[...], jnp.exp(rate_ref[...]), skip_ref[...])):
+                params_ref[place] = jnp.dot(
+                    value, wider, preferred_element_type=F32, precision=lax.Precision.HIGHEST)
+
+        def convolve(j):
+            return jnp.sum(
+                recent_ref[level, :, j].astype(F32)
+                * taps_ref[: taps_ref.shape[0] - 1, j, level, :].astype(F32)[None],
+                axis=1,
+            )
+
+        for j in range(3):
+            conv_ref[j] = convolve(j)
 
         each(dp - 1, lambda k: send_extra(level, k).wait_recv())
 
@@ -221,15 +260,13 @@
         both = fold(dp - 1, add_extra, extra_send[level, me].astype(F32))
         total = both[:, :LANES] + both[:, LANES:]
         scale = lax.rsqrt(total[:, LANES - 1 :] / features + EPS)
-        pick = lax.broadcasted_iota(jnp.int32, (LANES, cols), 0)
-        slot = lax.broadcasted_iota(jnp.int32, (LANES, cols), 1)
-        chosen = jnp.where(pick == col * heads + slot // head_dim, 1.0, 0.0).astype(BF16)
+        chosen = chosen_ref[...]
         high, rest = halves(total * scale)
         raw = jnp.dot(high, chosen, preferred_element_type=F32) + jnp.dot(
             rest, chosen, preferred_element_type=F32)
-        raw = raw + params_ref[level, 0:1, :]
+        raw = raw + params_ref[0, level : level + 1, :]
         size = jnp.maximum(raw, 0.0) + jnp.log1p(jnp.exp(-jnp.abs(raw)))
-        decay = jnp.exp(-size * params_ref[level, 1:2, :])
+        decay = jnp.exp(-size * params_ref[1, level : level + 1, :])
 
         def total_part(w):
             each(dp - 1, lambda k: send_part(level, w, k).wait_recv())
@@ -243,8 +280,8 @@
             u = total_part(w).astype(BF16)
             u_out[level, :, place * cols : (place + 1) * cols] = u
             return silu(
-                conv_ref[level, :, place * cols : (place + 1) * cols]
-                + u.astype(F32) * params_ref[level, 4 + place : 5 + place, :])
+                conv_ref[place]
+                + u.astype(F32) * taps_ref[taps_ref.shape[0] - 1, place, level : level + 1, :].astype(F32))
 
         bm = active(0, 1)
         cm = active(1, 2)
@@ -253,77 +290,88 @@
             dec_ref[h] = twice(decay[:, window], h % 2)
             bm_ref[h] = twice(bm[:, window], h % 2)
             cm_ref[h] = twice(cm[:, window], h % 2)
+        load_state(level).wait()
+        piece = 512
+        pieces = head_dim * span // piece
+
+        def across(ref, h):
+            return jnp.concatenate([ref[h]] * (piece // LANES), axis=1)
+
+        def consult(index, y):
+            window = pl.ds(pl.multiple_of(index * piece, piece), piece)
+            read = jnp.concatenate(
+                [state[level, h, :, window] * across(cm_ref, h) for h in range(heads)], axis=0)
+            return y + jnp.dot(
+                read.astype(BF16), gather[window, :], preferred_element_type=F32)
+
+        y = lax.fori_loop(0, pieces, consult, jnp.zeros((heads * own, LANES), F32))
         xv = active(2, 0)
         weighted = size * xv
+        inner = []
         for h in range(heads):
             window = slice(h // 2 * LANES, h // 2 * LANES + LANES)
             one = twice(weighted[:, window], h % 2)
             high = one.astype(BF16).astype(F32)
             wide_ref[h * own : (h + 1) * own, :] = jnp.where(low, high, one - high)
+            within = jnp.sum(
+                jnp.where(low, bm_ref[h] * cm_ref[h], 0.0), axis=1, keepdims=True)
+            inner.append(dec_ref[h] * y[h * own : (h + 1) * own] + one * within)
+        y = jnp.concatenate(
+            [jnp.where(low, inner[h], inner[h + 1]) for h in range(0, heads, 2)], axis=1)
+        y = y + params_ref[2, level : level + 1, :] * xv
+        gate = total_part(3)
+        gated_all[level, me] = (y * silu(gate) * gain_ref[level : level + 1, :]).astype(BF16)
+        each(dp - 1, lambda k: send_gated(level, k).start())
         wide = wide_ref[...].astype(BF16)
-        load_state(level).wait()
-        piece = 512
-
-        def advance(index, y):
-            start = pl.multiple_of(index * piece, piece)
-            window = pl.ds(start, piece)
+
+        def advance(index, carry):
+            window = pl.ds(pl.multiple_of(index * piece, piece), piece)
             grown = jnp.dot(wide, spread[:, window], preferred_element_type=F32)
-            read = []
             for h in range(heads):
-                def across(ref):
-                    return jnp.concatenate([ref[h]] * (piece // LANES), axis=1)
-
-                fresh = across(dec_ref) * state[level, h, :, window] + (
-                    grown[h * own : (h + 1) * own] * across(bm_ref))
-                state[level, h, :, window] = fresh
-                read.append(fresh * across(cm_ref))
-            read = jnp.concatenate(read, axis=0).astype(BF16)
-            return y + jnp.dot(read, gather[window, :], preferred_element_type=F32)
-
-        y = lax.fori_loop(
-            0, head_dim * span // piece, advance, jnp.zeros((heads * own, LANES), F32))
-        save_state(level).start()
-        y = jnp.concatenate(
-            [
-                jnp.where(low, y[h * own : (h + 1) * own], y[(h + 1) * own : (h + 2) * own])
-                for h in range(0, heads, 2)
-            ],
-            axis=1,
-        )
-        y = y + params_ref[level, 2:3, :] * xv
-        gate = total_part(3)
-        gated_all[level, me] = (y * silu(gate) * params_ref[level, 3:4, :]).astype(BF16)
-        each(dp - 1, lambda k: send_gated(level, k).start())
+                fresh_out[level, h, :, window] = (
+                    across(dec_ref, h) * state[level, h, :, window]
+                    + grown[h * own : (h + 1) * own] * across(bm_ref, h))
+            return carry
+
+        lax.fori_loop(0, pieces, advance, 0)
         load_out(level).wait()
         each(dp - 1, lambda k: send_gated(level, k).wait_recv())
         gated = gated_all[level].astype(F32).reshape(rows, cols)
         square = jnp.sum(gated * gated, axis=1, keepdims=True)
         mixed = jnp.dot(gated.astype(BF16), w_out[level], preferred_element_type=F32)
-        high = square.astype(BF16).astype(F32)
-        mixed_all[level, col, :, :width] = mixed.astype(BF16)
-        mixed_all[level, col, :, width:] = jnp.where(
-            lane_all < LANES // 2, high, square - high).astype(BF16)
+        mixed_all[level, col] = mixed.astype(BF16)
         each(tp - 1, lambda k: send_mixed(level, k).start())
+        cross = lax.broadcasted_iota(jnp.int32, (rows, rows), 0) == (
+            lax.broadcasted_iota(jnp.int32, (rows, rows), 1))
+        square_all[level, col, :, :rows] = jnp.broadcast_to(
+            jnp.sum(jnp.where(cross, square, 0.0), axis=0, keepdims=True), (8, rows))
+        each(tp - 1, lambda k: send_square(level, k).start())
+        each(tp - 1, lambda k: send_square(level, k).wait_recv())
+        square = fold(
+            tp,
+            lambda k, sum_in: sum_in + square_all[level, k, 0:1, :rows],
+            jnp.zeros((1, rows), F32),
+        )
+        scale = lax.rsqrt(square / (cols * tp) + EPS)
+        scale = jnp.sum(jnp.where(cross, scale, 0.0), axis=1, keepdims=True)
         each(tp - 1, lambda k: send_mixed(level, k).wait_recv())
         mixed = fold(
             tp,
             lambda k, sum_in: sum_in + mixed_all[level, k].astype(F32),
-            jnp.zeros((rows, width + LANES), F32),
-        )
-        square = mixed[:, width : width + 1] + mixed[:, width + LANES - 1 :]
-        scale = lax.rsqrt(square / (cols * tp) + EPS)
-        fresh_x = (x_ref[...] + scale * mixed[:, :width]).astype(BF16)
+            jnp.zeros((rows, width), F32),
+        )
+        fresh_x = (x_ref[...] + scale * mixed).astype(BF16)
         x_ref[...] = fresh_x.astype(F32)
         if level == layers - 1:
             tokens_out[...] = fresh_x
 
     for level in range(layers):
-        save_state(level).wait()
         each(dp - 1, lambda k: send_extra(level, k).wait_send())
         for w in range(4):
             each(dp - 1, lambda k: send_part(level, w, k).wait_send())
         each(dp - 1, lambda k: send_gated(level, k).wait_send())
         each(tp - 1, lambda k: send_mixed(level, k).wait_send())
+        each(tp - 1, lambda k: send_square(level, k).wait_send())
 
 
 def per_device(
@@ -354,23 +402,6 @@
     dims = (layers, dp, tp, own, cols, heads, head_dim, span, features, width)
     rows = tokens.shape[0]
 
-    def expand(value):
-        return jnp.repeat(value, head_dim, axis=1)[:, None]
-
-    taps = conv_taps.astype(F32)
-    params = jnp.concatenate(
-        [
-            expand(step_bias),
-            expand(jnp.exp(decay_log)),
-            expand(skip_gain),
-            gate_gain[:, None],
-            taps[:, -1],
-        ],
-        axis=1,
-    )
-    kept = jnp.sum(recent.astype(F32) * taps[:, None, :-1], axis=2).reshape(layers, own, 3 * cols)
-    step_weight = jnp.pad(w_step, ((0, 0), (0, 0), (0, LANES - w_step.shape[2])))
-    turned = states.transpose(0, 2, 1, 3)
     vmem = pl.BlockSpec(memory_space=pltpu.VMEM)
     anywhere = pl.BlockSpec(memory_space=pl.ANY)
     dma = pltpu.SemaphoreType.DMA
@@ -381,11 +412,11 @@
             jax.ShapeDtypeStruct((layers, heads, own, entries), F32),
             jax.ShapeDtypeStruct((layers, own, 3 * cols), BF16),
         ),
-        in_specs=[vmem] * 4 + [anywhere] * 7,
-        out_specs=(vmem, anywhere, vmem),
+        in_specs=[vmem] * 8 + [anywhere] * 7,
+        out_specs=(vmem, vmem, vmem),
         scratch_shapes=[
             pltpu.VMEM((layers, 4, width, cols), BF16),
-            pltpu.VMEM((layers, width, LANES), BF16),
+            pltpu.VMEM((layers, LANES, width), BF16),
             pltpu.VMEM((layers, cols, width), BF16),
             pltpu.VMEM((layers, heads, own, entries), F32),
             pltpu.VMEM((LANES, entries), BF16),
@@ -395,14 +426,17 @@
             pltpu.VMEM((layers, dp, own, 2 * LANES), BF16),
             pltpu.VMEM((layers, dp - 1, own, 2 * LANES), BF16),
             pltpu.VMEM((layers, dp, own, cols), BF16),
-            pltpu.VMEM((layers, tp, rows, width + LANES), BF16),
+            pltpu.VMEM((layers, tp, rows, width), BF16),
+            pltpu.VMEM((layers, tp, 8, -(-rows // LANES) * LANES), F32),
+            pltpu.VMEM((3, own, cols), F32),
+            pltpu.VMEM((3, layers, cols), F32),
+            pltpu.VMEM((LANES, cols), BF16),
             pltpu.VMEM((heads, own, LANES), F32),
             pltpu.VMEM((heads, own, LANES), F32),
             pltpu.VMEM((heads, own, LANES), F32),
             pltpu.VMEM((heads * own, LANES), F32),
             pltpu.VMEM((rows, width), F32),
             dma((layers, 4)),
-            dma((layers,)),
             dma((layers,)),
             dma((layers,)),
             dma((layers,)),
@@ -414,21 +448,27 @@
             dma((layers, dp - 1)),
             dma((layers, tp - 1)),
             dma((layers, tp - 1)),
+            dma((layers, tp - 1)),
+            dma((layers, tp - 1)),
         ],
         compiler_params=pltpu.CompilerParams(
-            collective_id=0, has_side_effects=True, vmem_limit_bytes=50 * 1024 * 1024),
+            collective_id=0, has_side_effects=True, vmem_limit_bytes=60 * 1024 * 1024),
     )(
         tokens,
         norm_gain,
-        params,
-        kept,
+        step_bias,
+        decay_log,
+        skip_gain,
+        gate_gain,
+        conv_taps.transpose(1, 2, 0, 3),
+        recent.transpose(0, 1, 3, 2, 4),
         w_value,
         w_inmap,
         w_readout,
         w_gate,
-        step_weight,
+        w_step.transpose(0, 2, 1),
         w_project,
-        turned,
+        states.transpose(0, 2, 1, 3),
     )
     next_states = fresh.transpose(0, 2, 1, 3)
     next_recent = jnp.concatenate(

time: 60.7 us -> 56.3 us (0.928)
  local copies, waits for them, and re-layouts: 8.48 us -> 5.68 us
  other arithmetic: 3.37 us -> 1.02 us
  Pallas kernels: 47.8 us -> 48.7 us
    unnamed x19 -> x6, local copies, waits for them, and re-layouts: 6.09 us -> 4.49 us
    reduce_sum x1 -> x0, other arithmetic: 1.41 us -> none  [per_device(): jnp.sum(recent.astype(F32) * taps[:, None, :-1], axis=2)]
    convert_element_type x1 -> x0, other arithmetic: 0.94 us -> none  [per_device(): taps = conv_taps.astype(F32)]
    reshape x1, local copies, waits for them, and re-layouts: 0.12 us -> 1.03 us  [per_device(): u.reshape(layers, own, 1, 3, cols)]
    broadcast_in_dim x4 -> x0, local copies, waits for them, and re-layouts: 0.9 us -> none  [the longest x3 0.9 us: expand(): return jnp.repeat(value, head_dim, axis=1)[:, None]]
    pallas_call x1, Pallas kernels: 47.8 us -> 48.7 us  [per_device(): pl.pallas_call(functools.partial(kernel, dims), out_shape=(jax.ShapeDtype...]
    exp x1 -> x0, local copies, waits for them, and re-layouts: 0.68 us -> none  [per_device(): jnp.exp(decay_log)]
where the time goes in v2:
time: 56.3 us; the launch traced here: 56.1 us
  Pallas kernels  48.7 us (87%)
  local copies, waits for them, and re-layouts  5.68 us (10%)
  other arithmetic  1.02 us (2%)
  between operations  0.68 us (1%)
    pallas_call x1, Pallas kernels, per_device(): pl.pallas_call(functools.partial(kernel, dims), out_shape=(jax.ShapeDtype...  48.7 us
    unnamed x6, local copies, waits for them, and re-layouts  4.49 us

profile of v2, /device:TPU:0, one launch (start us, length us, event | category | flops | bytes accessed | tf_op | source)
XLA Modules:
  0.0 56.1 jit_solution(4540522575638414450)
XLA Ops:
  0.6 0.0 copy-start
  0.6 48.7 %shard_map.166 = (bf16[64,512]{1,0:T(8,128)(2,1)}, f32[2,12,8,4096]{3,2,1,0:T(8,128)}, bf16[2,8,2304]{2,1,0:T(8,128)(2,1)}) custom-call(bf16[64,512]{1,0:T(8,128)(2,1)} %tokens_ref.1, f32[2,512]{1,0:T(2,128)} %norm_ref.1, f32[2,12]{1,0:T(2,128)} %bias_ref.1, f32[2,12]{1,0:T(2,128)} %rate_ref.1, f32[2,12]{1,0:T(2,128)} %skip_ref.1, f32[2,768]{1,0:T(2,128)} %gain_ref.1, ...), custom_call_target="tpu_custom_call" | custom-call | tf_op jit(solution)/shard_map/pallas_call | solution.py:408
  49.4 0.0 copy-start.1
  49.4 1.0 %copy.18 = bf16[2,8,1,3,768]{4,2,3,1,0:T(2,128)(2,1)S(1)} copy(bf16[2,8,1,3,768]{4,1,3,0,2:T(8,128)(2,1)} %bitcast.10) | data formatting | bytes 147456 | tf_op jit(solution)/shard_map/reshape | solution.py:475
  50.4 0.0 copy-done
  50.4 0.2 slice.3
  50.6 1.0 %pad_maximum_fusion = bf16[2,8,4,3,768]{4,2,3,1,0:T(4,128)(2,1)} fusion(bf16[2,8,1,3,768]{4,2,3,1,0:T(2,128)(2,1)S(1)} %copy.18, bf16[2,8,3,3,768]{4,2,3,1,0:T(4,128)(2,1)S(1)} %slice.3), kind=kLoop, calls=%fused_computation | loop fusion | flops 589824 | bytes 589824 | tf_op jit(solution)/shard_map/concatenate | solution.py:474
  51.6 0.0 copy-done.1
  51.6 0.6 %copy.21 = bf16[64,512]{1,0:T(8,128)(2,1)} copy(bf16[64,512]{1,0:T(8,128)(2,1)S(1)} %copy-done.1) | data formatting | bytes 131072
  52.2 3.9 %copy.22 = f32[2,8,12,4096]{3,1,2,0:T(8,128)} copy(f32[2,8,12,4096]{3,1,2,0:T(8,128)} %bitcast.6) | data formatting | bytes 6291456
Async XLA Ops:
  0.6 49.8 %copy-start = (bf16[2,8,4,3,768]{4,2,3,1,0:T(4,128)(2,1)S(1)}, bf16[2,8,4,3,768]{4,2,3,1,0:T(4,128)(2,1)}, u32[]{:S(2)}) copy-start(bf16[2,8,4,3,768]{4,2,3,1,0:T(4,128)(2,1)} %param.29) | copy-start | bytes 884740
  49.4 2.2 %copy-start.1 = (bf16[64,512]{1,0:T(8,128)(2,1)S(1)}, bf16[64,512]{1,0:T(8,128)(2,1)}, u32[]{:S(2)}) copy-start(bf16[64,512]{1,0:T(8,128)(2,1)} %get-tuple-element.12) | copy-start | bytes 196612

commit v3 on v2

--- a/solution.py
+++ b/solution.py
@@ -374,6 +374,31 @@
         each(tp - 1, lambda k: send_square(level, k).wait_send())
 
 
+def finish(
+    fresh_ref, tokens_ref, u_ref, recent_ref, tokens_out, fresh_hbm, recent_out, fresh_sem
+):
+    layers, heads = fresh_ref.shape[:2]
+    cols = recent_ref.shape[-1]
+
+    def save(level, h):
+        return pltpu.make_async_copy(
+            fresh_ref.at[level, h], fresh_hbm.at[level, h], fresh_sem.at[level, h])
+
+    for level in range(layers):
+        for h in range(heads):
+            save(level, h).start()
+    tokens_out[...] = tokens_ref[...]
+    for level in range(layers):
+        for j in range(3):
+            kept = recent_ref[level, :, j].astype(F32)
+            u = u_ref[level, :, j * cols : (j + 1) * cols].astype(F32)
+            recent_out[level, :, j] = jnp.concatenate(
+                [kept[:, 1:], u[:, None]], axis=1).astype(BF16)
+    for level in range(layers):
+        for h in range(heads):
+            save(level, h).wait()
+
+
 def per_device(
     dp,
     tp,
@@ -403,13 +428,14 @@
     rows = tokens.shape[0]
 
     vmem = pl.BlockSpec(memory_space=pltpu.VMEM)
-    anywhere = pl.BlockSpec(memory_space=pl.ANY)
+    anywhere = pl.BlockSpec(memory_space=pltpu.HBM)
+    turned = recent.transpose(0, 1, 3, 2, 4)
     dma = pltpu.SemaphoreType.DMA
     out_tokens, fresh, u = pl.pallas_call(
         functools.partial(kernel, dims),
         out_shape=(
             jax.ShapeDtypeStruct((rows, width), BF16),
-            jax.ShapeDtypeStruct((layers, heads, own, entries), F32),
+            pltpu.VMEM((layers, heads, own, entries), F32),
             jax.ShapeDtypeStruct((layers, own, 3 * cols), BF16),
         ),
         in_specs=[vmem] * 8 + [anywhere] * 7,
@@ -452,7 +478,7 @@
             dma((layers, tp - 1)),
         ],
         compiler_params=pltpu.CompilerParams(
-            collective_id=0, has_side_effects=True, vmem_limit_bytes=60 * 1024 * 1024),
+            collective_id=0, has_side_effects=True, vmem_limit_bytes=56 * 1024 * 1024),
     )(
         tokens,
         norm_gain,
@@ -461,7 +487,7 @@
         skip_gain,
         gate_gain,
         conv_taps.transpose(1, 2, 0, 3),
-        recent.transpose(0, 1, 3, 2, 4),
+        turned,
         w_value,
         w_inmap,
         w_readout,
@@ -470,9 +496,20 @@
         w_project,
         states.transpose(0, 2, 1, 3),
     )
+    out_tokens, fresh, kept = pl.pallas_call(
+        finish,
+        out_shape=(
+            jax.ShapeDtypeStruct(out_tokens.shape, BF16),
+            jax.ShapeDtypeStruct(fresh.shape, F32),
+            jax.ShapeDtypeStruct(turned.shape, BF16),
+        ),
+        in_specs=[vmem] * 4,
+        out_specs=(vmem, anywhere, vmem),
+        scratch_shapes=[dma((layers, heads))],
+        compiler_params=pltpu.CompilerParams(vmem_limit_bytes=16 * 1024 * 1024),
+    )(fresh, out_tokens, u, turned)
     next_states = fresh.transpose(0, 2, 1, 3)
-    next_recent = jnp.concatenate(
-        [recent[:, :, 1:], u.reshape(layers, own, 1, 3, cols)], axis=2)
+    next_recent = kept.transpose(0, 1, 3, 2, 4)
     return out_tokens, next_states, next_recent
 
 

time: 56.3 us -> 52.9 us (0.940)
  local copies, waits for them, and re-layouts: 5.68 us -> 1.72 us
  Pallas kernels: 48.7 us -> 50.3 us
  other arithmetic: 1.02 us -> 0 us
    unnamed x6, local copies, waits for them, and re-layouts: 4.49 us -> 1.72 us
    pallas_call x0 -> x1, Pallas kernels: none -> 2.58 us  [per_device(): pl.pallas_call(finish, out_shape=(jax.ShapeDtypeStruct(out_tokens.shape,...]
    reshape x1 -> x0, local copies, waits for them, and re-layouts: 1.03 us -> none  [per_device(): u.reshape(layers, own, 1, 3, cols)]
    pallas_call x1, Pallas kernels: 48.7 us -> 47.7 us  [per_device(): pl.pallas_call(functools.partial(kernel, dims), out_shape=(jax.ShapeDtype...]
    concatenate x1 -> x0, other arithmetic: 1.02 us -> none  [per_device(): jnp.concatenate([recent[:, :, 1:], u.reshape(layers, own, 1, 3, cols)], a...]
where the time goes in v3:
time: 52.9 us; the launch traced here: 52.7 us
  Pallas kernels  50.3 us (95%)
  local copies, waits for them, and re-layouts  1.72 us (3%)
  between operations  0.67 us (1%)
    pallas_call x1, Pallas kernels, per_device(): pl.pallas_call(functools.partial(kernel, dims), out_shape=(jax.ShapeDtype...  47.7 us
    pallas_call x1, Pallas kernels, per_device(): pl.pallas_call(finish, out_shape=(jax.ShapeDtypeStruct(out_tokens.shape,...  2.58 us
    unnamed x6, local copies, waits for them, and re-layouts  1.72 us

profile of v3, /device:TPU:0, one launch (start us, length us, event | category | flops | bytes accessed | tf_op | source)
XLA Modules:
  0.0 52.7 jit_solution(4111684131567452333)
XLA Ops:
  0.6 0.0 copy-start
  0.6 47.7 %shard_map.166 = (bf16[64,512]{1,0:T(8,128)(2,1)}, f32[2,12,8,4096]{3,2,1,0:T(8,128)S(1)}, bf16[2,8,2304]{2,1,0:T(8,128)(2,1)}) custom-call(bf16[64,512]{1,0:T(8,128)(2,1)} %tokens_ref.1, f32[2,512]{1,0:T(2,128)} %norm_ref.1, f32[2,12]{1,0:T(2,128)} %bias_ref.1, f32[2,12]{1,0:T(2,128)} %rate_ref.1, f32[2,12]{1,0:T(2,128)} %skip_ref.1, f32[2,768]{1,0:T(2,128)} %gain_ref.1, ...), custom_call_target="tpu_custom_call" | custom-call | tf_op jit(solution)/shard_map/pallas_call | solution.py:434
  48.3 0.0 copy-done
  48.4 0.0 copy-start.1
  48.4 0.9 %copy-done.1 = bf16[2,8,2304]{2,1,0:T(8,128)(2,1)S(1)} copy-done((bf16[2,8,2304]{2,1,0:T(8,128)(2,1)S(1)}, bf16[2,8,2304]{2,1,0:T(8,128)(2,1)}, u32[]{:S(2)}) %copy-start.1) | copy-done | bytes 73752
  49.2 0.0 copy-start.2
  49.2 0.8 %copy-done.2 = bf16[64,512]{1,0:T(8,128)(2,1)S(1)} copy-done((bf16[64,512]{1,0:T(8,128)(2,1)S(1)}, bf16[64,512]{1,0:T(8,128)(2,1)}, u32[]{:S(2)}) %copy-start.2) | copy-done | bytes 65560
  50.1 2.6 %shard_map.167 = (bf16[64,512]{1,0:T(8,128)(2,1)}, f32[2,12,8,4096]{3,2,1,0:T(8,128)}, bf16[2,8,3,4,768]{4,3,2,1,0:T(4,128)(2,1)}) custom-call(f32[2,12,8,4096]{3,2,1,0:T(8,128)S(1)} %get-tuple-element.9.fresh_ref, bf16[64,512]{1,0:T(8,128)(2,1)S(1)} %copy-done.2, bf16[2,8,2304]{2,1,0:T(8,128)(2,1)S(1)} %copy-done.1, bf16[2,8,3,4,768]{4,3,2,1,0:T(4,128)(2,1)S(1)} %bitcast.7), custom_call_target="tpu_custom_call" | custom-call | tf_op jit(solution)/shard_map/pallas_call | solution.py:499
Async XLA Ops:
  0.6 47.7 %copy-start = (bf16[2,8,4,3,768]{4,2,3,1,0:T(4,128)(2,1)S(1)}, bf16[2,8,4,3,768]{4,2,3,1,0:T(4,128)(2,1)}, u32[]{:S(2)}) copy-start(bf16[2,8,4,3,768]{4,2,3,1,0:T(4,128)(2,1)} %param.29) | copy-start | bytes 884740
  48.4 0.9 %copy-start.1 = (bf16[2,8,2304]{2,1,0:T(8,128)(2,1)S(1)}, bf16[2,8,2304]{2,1,0:T(8,128)(2,1)}, u32[]{:S(2)}) copy-start(bf16[2,8,2304]{2,1,0:T(8,128)(2,1)} %get-tuple-element.11.u_ref) | copy-start | bytes 221188
  49.2 0.8 %copy-start.2 = (bf16[64,512]{1,0:T(8,128)(2,1)S(1)}, bf16[64,512]{1,0:T(8,128)(2,1)}, u32[]{:S(2)}) copy-start(bf16[64,512]{1,0:T(8,128)(2,1)} %get-tuple-element.10.tokens_ref) | copy-start | bytes 196612
